TPU v7x, 32 devices: a whole 2x2x4 slice. The times are simulated.
32 devices in a mesh: kv: 8 (over z, y), tp: 4 (over x, core).
Axes of the slice: x: 2, y: 2, z: 4, core: 2. Of those that a mesh axis runs over, the one named last changes fastest.
Arguments:
- tokens: bfloat16 [16, 4096], P(None, 'tp'), may hold values from -6 to 6
- norm_gain: float32 [4096], P('tp'), may hold values from 0.1 to 1.9
- w_query: bfloat16 [4096, 32, 96], P('tp', 'kv'), as said below
- w_latent: bfloat16 [4096, 1024], P('tp', 'kv'), may hold values from -0.09375 to 0.09375
- w_rotary: bfloat16 [4096, 32], P('tp'), may hold values from -0.09375 to 0.09375
- latent_gain: float32 [1024], replicated, may hold values from 0.1 to 1.9
- w_key_up: bfloat16 [1024, 32, 64], P('tp', 'kv'), may hold values from -0.1875 to 0.1875
- w_value_up: bfloat16 [1024, 32, 128], replicated, may hold values from -0.1875 to 0.1875
- w_out: bfloat16 [4096, 4096], P('kv', 'tp'), may hold values from -0.09375 to 0.09375
- cache_latent: bfloat16 [16, 4096, 1024], P(None, ('kv', 'tp')), may hold values from -6 to 6
- cache_rotary: bfloat16 [16, 4096, 32], P(None, ('kv', 'tp')), may hold values from -6 to 6
- lengths: int32 [16], replicated, may hold values from 1024 to 4096
Outputs:
- mixed_out: bfloat16 [16, 4096], P(None, 'tp')
- new_latent: bfloat16 [16, 1024], P(None, ('kv', 'tp'))
- new_rotary: bfloat16 [16, 32], replicated
Inputs may be any that keep to these rules, and one draw needn't show every extreme that they name: `w_query`: finite.
All inputs are finite; a program needn't handle non-finite values.
Results may differ from a plain program's by a relative error of at most 0.012.
The roundings to bfloat16 on the way count: a program that leaves them out, or rounds other values in their place, can miss the bound.
Values may be sent and summed in bfloat16 or wider, within the bound.
A program may use at most 64 MiB of HBM per device.

v0:
```python
import jax
import jax.numpy as jnp
from jax import lax
from jax.sharding import PartitionSpec as P

THETA = 10000.0
EPS = 1e-06


def rotate(values, position):
    full_width = values.shape[-1]
    half_width = full_width // 2
    frequency = THETA ** (-jnp.arange(0, full_width, 2, dtype=jnp.float32) / full_width)
    angles = position.astype(jnp.float32)[:, None] * frequency[None, :]
    angles = angles.reshape((angles.shape[0],) + (1,) * (values.ndim - 2) + (half_width,))
    cosine = jnp.cos(angles)
    sine_part = jnp.sin(angles)
    first_half = values[..., :half_width]
    second_half = values[..., half_width:]
    return jnp.concatenate(
        [
            first_half * cosine - second_half * sine_part,
            first_half * sine_part + second_half * cosine,
        ],
        axis=-1,
    )


def value_product(latent_f, weight):
    high_part = latent_f.astype(jnp.bfloat16)
    low_part = (latent_f - high_part.astype(jnp.float32)).astype(jnp.bfloat16)
    return jnp.einsum(
        "bhr,rhv->bhv", high_part, weight, preferred_element_type=jnp.float32
    ) + jnp.einsum("bhr,rhv->bhv", low_part, weight, preferred_element_type=jnp.float32)


def shards(
    tokens,
    norm_gain,
    w_query,
    w_latent,
    w_rotary,
    latent_gain,
    w_key_up,
    w_value_up,
    w_out,
    cache_latent,
    cache_rotary,
    lengths,
):
    seq_count = tokens.shape[0]
    kv_count = lax.axis_size("kv")
    tp_count = lax.axis_size("tp")
    kv_index = lax.axis_index("kv")
    tp_index = lax.axis_index("tp")
    heads_dev = w_query.shape[1]
    head_count = heads_dev * kv_count
    latent_rank = cache_latent.shape[2]
    rope_width = cache_rotary.shape[2]
    nope_width = w_query.shape[2] - rope_width
    model_width = tokens.shape[1] * tp_count
    score_scale = w_query.shape[2] ** (-0.5)
    tokens_f = tokens.astype(jnp.float32)
    scaled = (tokens_f * norm_gain).astype(jnp.bfloat16)
    query_part = jnp.einsum("bd,dhn->bhn", scaled, w_query, preferred_element_type=jnp.float32)
    latent_part = jnp.dot(scaled, w_latent, preferred_element_type=jnp.float32)
    rotary_part = jnp.dot(scaled, w_rotary, preferred_element_type=jnp.float32)
    square_part = jnp.sum(tokens_f * tokens_f, axis=1)
    query_sum, latent_sum, rotary_sum, square_sum = lax.psum(
        (query_part, latent_part, rotary_part, square_part), "tp"
    )
    inverse = lax.rsqrt(square_sum / model_width + EPS)
    query_heads = (query_sum * inverse[:, None, None]).astype(jnp.bfloat16)
    compressed = (latent_sum * inverse[:, None]).astype(jnp.bfloat16)
    new_rotary = rotate(rotary_sum * inverse[:, None], lengths).astype(jnp.bfloat16)
    query_rope = rotate(query_heads[:, :, nope_width:].astype(jnp.float32), lengths).astype(
        jnp.bfloat16
    )
    query_latent = jnp.einsum(
        "bhn,rhn->bhr", query_heads[:, :, :nope_width], w_key_up, preferred_element_type=jnp.float32
    ).astype(jnp.bfloat16)
    rope_slice = rope_width // tp_count
    column_slice = compressed.shape[1] // tp_count
    rope_piece = lax.dynamic_slice_in_dim(query_rope, tp_index * rope_slice, rope_slice, 2)
    column_piece = lax.dynamic_slice_in_dim(compressed, tp_index * column_slice, column_slice, 1)
    got_latent, got_rope, got_columns = (
        lax.all_gather(query_latent[:, None], ("kv", "tp"), axis=1, tiled=True),
        lax.all_gather(rope_piece[:, None], ("kv", "tp"), axis=1, tiled=True),
        lax.all_gather(column_piece[:, None], ("kv", "tp"), axis=1, tiled=True),
    )
    rank_slice = query_latent.shape[2]
    all_latent = got_latent.reshape(seq_count, kv_count, tp_count, heads_dev, rank_slice)
    all_latent = all_latent.transpose(0, 1, 3, 2, 4).reshape(seq_count, head_count, latent_rank)
    all_rope = got_rope.reshape(seq_count, kv_count, tp_count, heads_dev, rope_slice)
    all_rope = all_rope.transpose(0, 1, 3, 2, 4).reshape(seq_count, head_count, rope_width)
    fresh_f = got_columns.reshape(seq_count, latent_rank).astype(jnp.float32)
    new_latent = (
        fresh_f * lax.rsqrt(jnp.mean(fresh_f * fresh_f, axis=1, keepdims=True) + EPS) * latent_gain
    ).astype(jnp.bfloat16)
    new_latent_f = new_latent.astype(jnp.float32)
    own_score = (
        jnp.einsum("bhr,br->bh", all_latent, new_latent, preferred_element_type=jnp.float32)
        + jnp.einsum("bhq,bq->bh", all_rope, new_rotary, preferred_element_type=jnp.float32)
    ) * score_scale
    pos_dev = cache_latent.shape[1]
    first_pos = (kv_index * tp_count + tp_index) * pos_dev
    position = first_pos + jnp.arange(pos_dev, dtype=jnp.int32)
    valid = position[None, :] < lengths[:, None]
    scores = (
        jnp.einsum("bhr,bpr->bhp", all_latent, cache_latent, preferred_element_type=jnp.float32)
        + jnp.einsum("bhq,bpq->bhp", all_rope, cache_rotary, preferred_element_type=jnp.float32)
    ) * score_scale
    masked = jnp.where(valid[:, None, :], scores, -jnp.inf)
    local_top = jnp.maximum(jnp.max(masked, axis=2), own_score)
    top_score = lax.pmax(local_top, ("kv", "tp"))
    weights = jnp.where(valid[:, None, :], jnp.exp(scores - top_score[:, :, None]), 0.0)
    total_part = jnp.sum(weights, axis=2)
    summed_part = jnp.einsum(
        "bhp,bpr->bhr",
        weights.astype(jnp.bfloat16),
        cache_latent,
        preferred_element_type=jnp.float32,
    )
    own_weight = jnp.exp(own_score - top_score)
    block_own = lax.dynamic_slice_in_dim(own_weight, kv_index * heads_dev, heads_dev, 1)
    value_block_weight = lax.dynamic_slice_in_dim(w_value_up, kv_index * heads_dev, heads_dev, 1)
    totals, summed = lax.psum((total_part, summed_part), ("kv", "tp"))
    block_sum = lax.dynamic_slice_in_dim(summed, kv_index * heads_dev, heads_dev, 1)
    block_total = lax.dynamic_slice_in_dim(totals, kv_index * heads_dev, heads_dev, 1)
    latent_out = (block_sum + block_own[:, :, None] * new_latent_f[:, None, :]) / (
        block_total + block_own
    )[:, :, None]
    head_out = value_product(latent_out, value_block_weight).astype(jnp.bfloat16)
    out_part = jnp.dot(head_out.reshape(seq_count, -1), w_out, preferred_element_type=jnp.float32)
    mixed_out = lax.psum(out_part, "kv").astype(jnp.bfloat16)
    latent_width = latent_rank // (kv_count * tp_count)
    latent_piece = lax.dynamic_slice_in_dim(
        new_latent, (kv_index * tp_count + tp_index) * latent_width, latent_width, 1
    )
    return (mixed_out, latent_piece, new_rotary)


def solution(mesh):
    placed = (
        P(None, "tp"),
        P("tp"),
        P("tp", "kv", None),
        P("tp", "kv"),
        P("tp", None),
        P(),
        P("tp", "kv", None),
        P(),
        P("kv", "tp"),
        P(None, ("kv", "tp"), None),
        P(None, ("kv", "tp"), None),
        P(),
    )
    return jax.shard_map(
        shards,
        mesh=mesh,
        in_specs=placed,
        out_specs=(P(None, "tp"), P(None, ("kv", "tp")), P()),
        check_vma=False,
    )
```

profile of v0, /device:TPU:0, one launch (start us, length us, event | category | flops | bytes accessed | tf_op | source)
XLA Modules:
  0.0 341.0 jit_solution(9099277364081239508)
XLA Ops:
  7.2 1.0 fusion.15
  8.2 1.5 fusion.20
  9.7 1.0 fusion.22
  10.7 1.1 fusion.24
  11.9 13.4 %all-reduce = (f32[16,4,96]{2,0,1:T(8,128)S(1)}, f32[16]{0:T(128)S(1)}, f32[16,128]{1,0:T(8,128)S(1)}, f32[16,32]{1,0:T(8,128)S(1)}) all-reduce(f32[16,4,96]{2,0,1:T(8,128)S(1)} %fusion.20, f32[16]{0:T(128)S(1)} %fusion.15, f32[16,128]{1,0:T(8,128)S(1)} %fusion.24, f32[16,32]{1,0:T(8,128)S(1)} %fusion.22), channel_id=1, replica_groups=mesh['kv'=8,'tp'=4] {'tp'}, use_global_device_ids=true, to_apply=%region_0.0 | all-reduce | flops 8720 | bytes 69760 | tf_op jit(solution)/shard_map/psum | solution.py:69
  25.3 1.7 fusion.1
  27.1 0.7 convert_element_type.81
  28.3 41.5 %all-gather.1 = bf16[16,128,8]{0,2,1:T(8,128)(2,1)S(1)} all-gather(bf16[16,4,8]{0,2,1:T(8,128)(2,1)S(1)} %copy.48), channel_id=3, replica_groups=mesh['kv'=8,'tp'=4] {'kv','tp'}, dimensions={1}, use_global_device_ids=true | all-gather | bytes 33792 | tf_op jit(solution)/shard_map/all_gather | solution.py:88
  70.1 37.0 %all-gather.3 = bf16[32,32,16]{1,2,0:T(8,128)(2,1)S(1)} all-gather(bf16[1,32,16]{1,2,0:T(8,128)(2,1)S(1)} %get-tuple-element.20), channel_id=4, replica_groups=mesh['kv'=8,'tp'=4] {'kv','tp'}, dimensions={0}, use_global_device_ids=true | all-gather | bytes 33792 | tf_op jit(solution)/shard_map/all_gather | solution.py:89
  107.5 0.7 broadcast_compare_fusion
  108.5 2.0 copy.75
  110.6 0.8 reshape.151
  111.3 3.7 %fusion.41 = f32[16,32,128]{2,1,0:T(8,128)S(1)} fusion(bf16[16,32,1024]{2,1,0:T(8,128)(2,1)S(1)} %reshape.151, bf16[16,128,1024]{2,1,0:T(8,128)(2,1)} %param.21), kind=kOutput, calls=%fused_computation.71 | convolution fusion | flops 134217728 | bytes 5505024 | tf_op jit(solution)/shard_map/bhr,bpr->bhp/dot_general | solution.py:110
  115.7 37.0 %pmax.7 = f32[16,32]{1,0:T(8,128)S(1)} all-reduce(f32[16,32]{1,0:T(8,128)S(1)} %get-tuple-element.11), channel_id=1, replica_groups=mesh['kv'=8,'tp'=4] {'kv','tp'}, use_global_device_ids=true, to_apply=%region_7.8 | all-reduce | flops 512 | bytes 4096 | tf_op jit(solution)/shard_map/pmax | solution.py:115
  152.7 2.9 fusion.9
  155.6 2.5 copy.52
  158.2 0.7 pad_maximum_fusion
  158.9 0.7 dynamic-slice_bitcast_fusion
  159.5 2.1 constant_dynamic-slice_fusion
  161.9 42.7 %psum.54 = f32[16,32]{1,0:T(8,128)S(1)} all-reduce(f32[16,32]{1,0:T(8,128)S(1)} %fusion.7), channel_id=1, replica_groups=mesh['kv'=8,'tp'=4] {'kv','tp'}, use_global_device_ids=true, to_apply=%region_10.11 | all-reduce | flops 512 | bytes 4096 | tf_op jit(solution)/shard_map/psum | solution.py:127
  204.8 89.8 %all-reduce.3.cloned.1.call-done = f32[16,32,1024]{2,0,1:T(8,128)} async-done(((f32[16,32,1024]{2,0,1:T(8,128)}), f32[16,32,1024]{2,0,1:T(8,128)}) %all-reduce.3.cloned.1.call-update) | async-done | bytes 2097168 | tf_op jit(solution)/shard_map/psum | solution.py:127
  294.6 1.3 fusion.4
  295.9 1.3 fusion.3
  297.4 36.8 %psum.55 = bf16[16,1024]{1,0:T(8,128)(2,1)} all-reduce(f32[16,1024]{1,0:T(8,128)S(1)} %fusion.27), channel_id=1, replica_groups=mesh['kv'=8,'tp'=4] {'kv'}, use_global_device_ids=true, to_apply=%region_11.12 | all-reduce | flops 16384 | bytes 98304 | tf_op jit(solution)/shard_map/psum | solution.py:135
  (38 shorter events, 3.1 us)
Async XLA Ops:
  7.2 290.0 %copy-start = (bf16[512,1024]{1,0:T(8,128)(2,1)S(1)}, bf16[512,1024]{1,0:T(8,128)(2,1)}, u32[]{:S(2)}) copy-start(bf16[512,1024]{1,0:T(8,128)(2,1)} %param.20) | copy-start | bytes 3145732
  7.2 101.2 %copy-start.2 = (f32[1024]{0:T(1024)S(1)}, f32[1024]{0:T(1024)}, u32[]{:S(2)}) copy-start(f32[1024]{0:T(1024)} %param.17) | copy-start | bytes 12292
  7.2 101.3 %all-gather.6.cloned.1.call-start = ((), (), s32[]{:S(2)}) async-start(), calls=%async_computation.1 | async-start | bytes 1081344 | tf_op jit(solution)/shard_map/all_gather | solution.py:87
  27.0 267.6 %all-reduce.3.cloned.1.call-start = ((), (), s32[]{:S(2)}) async-start(), calls=%async_computation | async-start | bytes 4194304 | tf_op jit(solution)/shard_map/psum | solution.py:127
  110.5 4.9 %copy-start.1 = (bf16[16,128,32]{1,2,0:T(8,128)(2,1)S(1)}, bf16[16,128,32]{1,2,0:T(8,128)(2,1)}, u32[]{:S(2)}) copy-start(bf16[16,128,32]{1,2,0:T(8,128)(2,1)} %param.22) | copy-start | bytes 393220
Sparse Core Ops, SparseCore 0:
  27.1 54.0 all-gather.5
  158.3 136.2 all-reduce.2
where the time goes:
time: 342 us; the launch traced here: 341 us
  blocking collectives  208 us (61%)
  waiting for transfers between devices  89.9 us (26%)
  matrix products  15.6 us (5%)
  between operations  14.2 us (4%)
  local copies, waits for them, and re-layouts  8.86 us (3%)
  other arithmetic  4.22 us (1%)
    psum x1, waiting for transfers between devices, shards(): totals, summed = lax.psum((total_part, summed_part), ('kv', 'tp'))  89.8 us
    psum x1, blocking collectives, shards(): totals, summed = lax.psum((total_part, summed_part), ('kv', 'tp'))  42.7 us
    all_gather x1, blocking collectives, shards(): lax.all_gather(rope_piece[:, None], ('kv', 'tp'), axis=1, tiled=True)  41.5 us
    all_gather x1, blocking collectives, shards(): lax.all_gather(column_piece[:, None], ('kv', 'tp'), axis=1, tiled=True)  37 us
    pmax x1, blocking collectives, shards(): top_score = lax.pmax(local_top, ('kv', 'tp'))  37 us
    psum x1, blocking collectives, shards(): mixed_out = lax.psum(out_part, 'kv').astype(jnp.bfloat16)  36.8 us
    psum x1, blocking collectives, shards(): lax.psum((query_part, latent_part, rotary_part, square_part), 'tp')  13.4 us
  transfers between devices with their start and end apart: 2, of which 1 were waited for; matrix products, arithmetic and copies ran while one was open for 2% of the time, Pallas kernels for 0%

commit v1 on v0

--- a/solution.py
+++ b/solution.py
@@ -124,7 +124,7 @@
     own_weight = jnp.exp(own_score - top_score)
     block_own = lax.dynamic_slice_in_dim(own_weight, kv_index * heads_dev, heads_dev, 1)
     value_block_weight = lax.dynamic_slice_in_dim(w_value_up, kv_index * heads_dev, heads_dev, 1)
-    totals, summed = lax.psum((total_part, summed_part), ("kv", "tp"))
+    totals, summed = lax.psum(lax.psum((total_part, summed_part), "kv"), "tp")
     block_sum = lax.dynamic_slice_in_dim(summed, kv_index * heads_dev, heads_dev, 1)
     block_total = lax.dynamic_slice_in_dim(totals, kv_index * heads_dev, heads_dev, 1)
     latent_out = (block_sum + block_own[:, :, None] * new_latent_f[:, None, :]) / (

time: 342 us -> 364 us (1.064)
  waiting for transfers between devices: 89.9 us -> 128 us
  blocking collectives: 208 us -> 193 us
    psum x1 -> x2, waiting for transfers between devices: 89.8 us -> 128 us  [shards(): totals, summed = lax.psum(lax.psum((total_part, summed_part), 'kv'), 'tp')]
    psum x1 -> x2, blocking collectives: 42.7 us -> 25.6 us  [shards(): totals, summed = lax.psum(lax.psum((total_part, summed_part), 'kv'), 'tp')]
  transfers between devices with their start and end apart: 2 -> 3, of which waited for: 1 -> 2; matrix products, arithmetic and copies ran while one was open for 2% -> 2% of each run, Pallas kernels for 0% -> 0%
where the time goes in v1:
time: 364 us; the launch traced here: 363 us
  blocking collectives  193 us (53%)
  waiting for transfers between devices  128 us (35%)
  matrix products  15.6 us (4%)
  between operations  13.9 us (4%)
  local copies, waits for them, and re-layouts  8.86 us (2%)
  other arithmetic  4.23 us (1%)
    psum x2, waiting for transfers between devices, shards(): totals, summed = lax.psum(lax.psum((total_part, summed_part), 'kv'), 'tp')  128 us
    all_gather x1, blocking collectives, shards(): lax.all_gather(rope_piece[:, None], ('kv', 'tp'), axis=1, tiled=True)  41.5 us
    psum x1, blocking collectives, shards(): mixed_out = lax.psum(out_part, 'kv').astype(jnp.bfloat16)  38.1 us
    all_gather x1, blocking collectives, shards(): lax.all_gather(column_piece[:, None], ('kv', 'tp'), axis=1, tiled=True)  37 us
    pmax x1, blocking collectives, shards(): top_score = lax.pmax(local_top, ('kv', 'tp'))  37 us
    psum x2, blocking collectives, shards(): totals, summed = lax.psum(lax.psum((total_part, summed_part), 'kv'), 'tp')  25.6 us
    psum x1, blocking collectives, shards(): lax.psum((query_part, latent_part, rotary_part, square_part), 'tp')  13.4 us
  transfers between devices with their start and end apart: 3, of which 2 were waited for; matrix products, arithmetic and copies ran while one was open for 2% of the time, Pallas kernels for 0%

profile of v1, /device:TPU:0, one launch (start us, length us, event | category | flops | bytes accessed | tf_op | source)
XLA Modules:
  0.0 362.9 jit_solution(10456254263090970089)
XLA Ops:
  7.2 1.0 fusion.15
  8.2 1.5 fusion.20
  9.7 1.0 fusion.22
  10.7 1.1 fusion.24
  11.9 13.4 %all-reduce = (f32[16,4,96]{2,0,1:T(8,128)S(1)}, f32[16]{0:T(128)S(1)}, f32[16,128]{1,0:T(8,128)S(1)}, f32[16,32]{1,0:T(8,128)S(1)}) all-reduce(f32[16,4,96]{2,0,1:T(8,128)S(1)} %fusion.20, f32[16]{0:T(128)S(1)} %fusion.15, f32[16,128]{1,0:T(8,128)S(1)} %fusion.24, f32[16,32]{1,0:T(8,128)S(1)} %fusion.22), channel_id=1, replica_groups=mesh['kv'=8,'tp'=4] {'tp'}, use_global_device_ids=true, to_apply=%region_0.0 | all-reduce | flops 8720 | bytes 69760 | tf_op jit(solution)/shard_map/psum | solution.py:69
  25.3 1.7 fusion.1
  28.3 41.5 %all-gather.1 = bf16[16,128,8]{0,2,1:T(8,128)(2,1)S(1)} all-gather(bf16[16,4,8]{0,2,1:T(8,128)(2,1)S(1)} %copy.48), channel_id=3, replica_groups=mesh['kv'=8,'tp'=4] {'kv','tp'}, dimensions={1}, use_global_device_ids=true | all-gather | bytes 33792 | tf_op jit(solution)/shard_map/all_gather | solution.py:88
  70.1 37.0 %all-gather.3 = bf16[32,32,16]{1,2,0:T(8,128)(2,1)S(1)} all-gather(bf16[1,32,16]{1,2,0:T(8,128)(2,1)S(1)} %get-tuple-element.20), channel_id=4, replica_groups=mesh['kv'=8,'tp'=4] {'kv','tp'}, dimensions={0}, use_global_device_ids=true | all-gather | bytes 33792 | tf_op jit(solution)/shard_map/all_gather | solution.py:89
  107.5 0.7 broadcast_compare_fusion
  108.5 2.0 copy.75
  110.6 0.8 reshape.151
  111.3 3.7 %fusion.41 = f32[16,32,128]{2,1,0:T(8,128)S(1)} fusion(bf16[16,32,1024]{2,1,0:T(8,128)(2,1)S(1)} %reshape.151, bf16[16,128,1024]{2,1,0:T(8,128)(2,1)} %param.21), kind=kOutput, calls=%fused_computation.71 | convolution fusion | flops 134217728 | bytes 5505024 | tf_op jit(solution)/shard_map/bhr,bpr->bhp/dot_general | solution.py:110
  115.7 37.0 %pmax.7 = f32[16,32]{1,0:T(8,128)S(1)} all-reduce(f32[16,32]{1,0:T(8,128)S(1)} %get-tuple-element.11), channel_id=1, replica_groups=mesh['kv'=8,'tp'=4] {'kv','tp'}, use_global_device_ids=true, to_apply=%region_7.8 | all-reduce | flops 512 | bytes 4096 | tf_op jit(solution)/shard_map/pmax | solution.py:115
  152.7 2.9 fusion.9
  155.6 2.5 copy.52
  158.2 103.9 %all-reduce.4.cloned.1.call-done = f32[16,32,1024]{2,0,1:T(8,128)} async-done(((f32[16,32,1024]{2,0,1:T(8,128)}), f32[16,32,1024]{2,0,1:T(8,128)}) %all-reduce.4.cloned.1.call-update) | async-done | bytes 2097168 | tf_op jit(solution)/shard_map/psum | solution.py:127
  262.1 0.7 pad_maximum_fusion
  263.5 2.1 constant_dynamic-slice_fusion
  265.9 19.9 %psum.69 = f32[16,32]{1,0:T(8,128)S(1)} all-reduce(f32[16,32]{1,0:T(8,128)S(1)} %fusion.7), channel_id=1, replica_groups=mesh['kv'=8,'tp'=4] {'kv'}, use_global_device_ids=true, to_apply=%region_11.12 | all-reduce | flops 512 | bytes 4096 | tf_op jit(solution)/shard_map/psum | solution.py:127
  285.8 5.8 %psum.70 = f32[16,32]{1,0:T(8,128)S(1)} all-reduce(f32[16,32]{1,0:T(8,128)S(1)} %psum.69), channel_id=1, replica_groups=mesh['kv'=8,'tp'=4] {'tp'}, use_global_device_ids=true, to_apply=%region_12.13 | all-reduce | flops 512 | bytes 4096 | tf_op jit(solution)/shard_map/psum | solution.py:127
  291.8 23.7 %all-reduce.6.cloned.1.call-done = f32[16,32,1024]{2,0,1:T(8,128)} async-done(((f32[16,32,1024]{2,0,1:T(8,128)}), f32[16,32,1024]{2,0,1:T(8,128)}) %all-reduce.6.cloned.1.call-update) | async-done | bytes 2097168 | tf_op jit(solution)/shard_map/psum | solution.py:127
  315.4 1.3 fusion.4
  316.7 1.3 fusion.3
  318.2 38.1 %psum.71 = bf16[16,1024]{1,0:T(8,128)(2,1)} all-reduce(f32[16,1024]{1,0:T(8,128)S(1)} %fusion.27), channel_id=1, replica_groups=mesh['kv'=8,'tp'=4] {'kv'}, use_global_device_ids=true, to_apply=%region_13.14 | all-reduce | flops 16384 | bytes 98304 | tf_op jit(solution)/shard_map/psum | solution.py:135
  (42 shorter events, 4.5 us)
Async XLA Ops:
  7.2 310.8 %copy-start = (bf16[512,1024]{1,0:T(8,128)(2,1)S(1)}, bf16[512,1024]{1,0:T(8,128)(2,1)}, u32[]{:S(2)}) copy-start(bf16[512,1024]{1,0:T(8,128)(2,1)} %param.20) | copy-start | bytes 3145732
  7.2 101.2 %copy-start.2 = (f32[1024]{0:T(1024)S(1)}, f32[1024]{0:T(1024)}, u32[]{:S(2)}) copy-start(f32[1024]{0:T(1024)} %param.17) | copy-start | bytes 12292
  7.2 101.3 %all-gather.6.cloned.1.call-start = ((), (), s32[]{:S(2)}) async-start(), calls=%async_computation.2 | async-start | bytes 1081344 | tf_op jit(solution)/shard_map/all_gather | solution.py:87
  27.0 235.1 %all-reduce.4.cloned.1.call-start = ((), (), s32[]{:S(2)}) async-start(), calls=%async_computation | async-start | bytes 4194304 | tf_op jit(solution)/shard_map/psum | solution.py:127
  110.5 4.9 %copy-start.1 = (bf16[16,128,32]{1,2,0:T(8,128)(2,1)S(1)}, bf16[16,128,32]{1,2,0:T(8,128)(2,1)}, u32[]{:S(2)}) copy-start(bf16[16,128,32]{1,2,0:T(8,128)(2,1)} %param.22) | copy-start | bytes 393220
  158.2 157.3 %all-reduce.6.cloned.1.call-start = ((), (), s32[]{:S(2)}) async-start(), calls=%async_computation.1 | async-start | bytes 4194304 | tf_op jit(solution)/shard_map/psum | solution.py:127
Sparse Core Ops, SparseCore 0:
  27.1 54.0 all-gather.5
  158.3 103.7 all-reduce.3
  264.5 50.9 all-reduce.5
